TPU v7x, 32 devices: a whole 2x2x4 slice. The times are simulated.
32 devices in a mesh: sp: 8 (over z, y), tp: 4 (over x, core).
Axes of the slice: x: 2, y: 2, z: 4, core: 2. Of those that a mesh axis runs over, the one named last changes fastest.
Arguments:
- inputs: bfloat16 [8192, 2048], P('sp'), may hold values from -6 to 6
- norm_gain: float32 [3, 2048], replicated, may hold values from 0.1 to 1.9
- query_weight: bfloat16 [3, 2048, 1024], P(None, 'sp', 'tp'), may hold values from -64 to 64
- key_weight: bfloat16 [3, 2048, 512], P(None, 'sp', 'tp'), may hold values from -4 to 4
- value_weight: bfloat16 [3, 2048, 512], P(None, 'sp', 'tp'), may hold values from -0.125 to 0.125
- output_weight: bfloat16 [3, 2048, 1024], P(None, 'sp', 'tp'), may hold values from -0.1875 to 0.1875
- sink_logit: float32 [3, 16], P(None, 'tp'), may hold values from 2 to 7
- final_gain: float32 [2048], replicated, may hold values from 0.1 to 1.9
Outputs:
- result: float32 [8192, 2048], P(('sp', 'tp'))
All inputs are finite; a program needn't handle non-finite values.
Results may differ from a plain program's by a relative error of at most 0.015.
Values may be sent and summed in bfloat16 or wider, within the bound.
A program may use at most 64 MiB of HBM per device.

v0:
```python
import jax
import jax.numpy as jnp
from jax import lax
from jax.sharding import PartitionSpec as P

D = 2048
HEAD_DIM = 64
WINDOW = 128
LAYERS = 3
EPS = 1e-06


def extended_2(block, sides, width):
    for axis, dim in sides:
        count = lax.axis_size(axis)
        forward = [(i, i + 1) for i in range(count - 1)]
        backward = [(target, source) for source, target in forward]
        low = lax.ppermute(
            lax.slice_in_dim(block, block.shape[dim] - width, None, axis=dim), axis, forward
        )
        high = lax.ppermute(lax.slice_in_dim(block, 0, width, axis=dim), axis, backward)
        block = jnp.concatenate([low, block, high], axis=dim)
    return block


def norm_rows(values, gain):
    wide_values = values.astype(jnp.float32)
    inv_root = lax.rsqrt(jnp.mean(wide_values * wide_values, axis=-1, keepdims=True) + EPS)
    return wide_values * inv_root * gain


def rotate(values, places):
    half_dim = values.shape[-1] // 2
    inverse = 10000.0 ** (-jnp.arange(half_dim).astype(jnp.float32) / half_dim)
    angles = places[:, None] * inverse[None, :]
    cosine_table = jnp.cos(angles)[:, None, :]
    sine_table = jnp.sin(angles)[:, None, :]
    front_half = values[..., :half_dim]
    back_half = values[..., half_dim:]
    return jnp.concatenate(
        [
            front_half * cosine_table - back_half * sine_table,
            back_half * cosine_table + front_half * sine_table,
        ],
        axis=-1,
    )


def attend(queries, key_rows, value_rows, sink_row, allowed):
    scores = jnp.einsum(
        "qkgd,skd->kgqs", queries, key_rows, preferred_element_type=jnp.float32
    ) * queries.shape[-1] ** (-0.5)
    scores = jnp.where(allowed[None, None], scores, -jnp.inf)
    sink_col = sink_row[:, :, None]
    largest = jnp.maximum(jnp.max(scores, axis=-1), sink_col)
    powers = jnp.exp(scores - largest[..., None])
    denominator = jnp.sum(powers, axis=-1) + jnp.exp(sink_col - largest)
    weights = (powers / denominator[..., None]).astype(jnp.bfloat16)
    blended = jnp.einsum("kgqs,skd->qkgd", weights, value_rows, preferred_element_type=jnp.float32)
    return blended.astype(jnp.bfloat16)


def shards(
    inputs, norm_gain, query_weight, key_weight, value_weight, output_weight, sink_logit, final_gain
):
    tokens = inputs.shape[0]
    local_heads = query_weight.shape[2] // HEAD_DIM
    local_groups = key_weight.shape[2] // HEAD_DIM
    per_group = local_heads // local_groups
    kv_cols = local_groups * HEAD_DIM
    offset = lax.axis_index("sp") * tokens
    seq_total = tokens * lax.axis_size("sp")
    query_pos = offset + jnp.arange(tokens, dtype=jnp.int32)
    places = query_pos.astype(jnp.float32)
    key_pos = offset - WINDOW + jnp.arange(tokens + 2 * WINDOW, dtype=jnp.int32)
    allowed = (
        (jnp.abs(key_pos[None, :] - query_pos[:, None]) <= WINDOW)
        & (key_pos[None, :] >= 0)
        & (key_pos[None, :] < seq_total)
    )
    whole_query, whole_key, whole_value, whole_out = (
        lax.all_gather(query_weight, "sp", axis=1, tiled=True),
        lax.all_gather(key_weight, "sp", axis=1, tiled=True),
        lax.all_gather(value_weight, "sp", axis=1, tiled=True),
        lax.all_gather(output_weight, "sp", axis=1, tiled=True),
    )
    current = inputs
    final_rows = inputs
    for layer in range(LAYERS):
        normed = norm_rows(current, norm_gain[layer]).astype(jnp.bfloat16)
        query_raw = jnp.dot(normed, whole_query[layer], preferred_element_type=jnp.float32)
        key_raw = jnp.dot(normed, whole_key[layer], preferred_element_type=jnp.float32)
        value_raw = jnp.dot(normed, whole_value[layer], preferred_element_type=jnp.float32)
        out_weight = whole_out[layer]
        queries = rotate(
            (query_raw * float(D) ** (-0.5)).reshape(tokens, local_heads, HEAD_DIM), places
        ).astype(jnp.bfloat16)
        key_rot = rotate(
            (key_raw * float(D) ** (-0.5)).reshape(tokens, local_groups, HEAD_DIM), places
        ).astype(jnp.bfloat16)
        packed = jnp.concatenate(
            [key_rot.reshape(tokens, kv_cols), value_raw.astype(jnp.bfloat16)], axis=1
        )
        extended = extended_2(packed, (("sp", 0),), WINDOW)
        key_rows = extended[:, :kv_cols].reshape(-1, local_groups, HEAD_DIM)
        value_all = extended[:, kv_cols:].reshape(-1, local_groups, HEAD_DIM)
        sink_row = sink_logit[layer].reshape(local_groups, per_group)
        attended = attend(
            queries.reshape(tokens, local_groups, per_group, HEAD_DIM),
            key_rows,
            value_all,
            sink_row,
            allowed,
        )
        attended = attended.reshape(tokens, local_heads * HEAD_DIM)

        def project():
            return lax.dot_general(
                attended, out_weight, (((1,), (1,)), ((), ())), preferred_element_type=jnp.float32
            )

        if layer < LAYERS - 1:
            share_rows = lax.psum_scatter(project(), "tp", scatter_dimension=0, tiled=True).astype(
                jnp.bfloat16
            )
            current = lax.all_gather(share_rows, "tp", axis=0, tiled=True)
        else:
            final_rows = lax.psum_scatter(
                project().astype(jnp.bfloat16), "tp", scatter_dimension=0, tiled=True
            )
    return norm_rows(final_rows, final_gain)


def solution(mesh):
    in_specs = (
        P("sp", None),
        P(),
        P(None, "sp", "tp"),
        P(None, "sp", "tp"),
        P(None, "sp", "tp"),
        P(None, "sp", "tp"),
        P(None, "tp"),
        P(),
    )
    out_specs = P(("sp", "tp"), None)
    return jax.shard_map(shards, mesh=mesh, in_specs=in_specs, out_specs=out_specs, check_vma=False)
```

profile of v0, /device:TPU:0, one launch (start us, length us, event | category | flops | bytes accessed | tf_op | source)
XLA Modules:
  0.0 580.5 jit_solution(9668719352871353835)
XLA Ops:
  10.4 3.3 fusion.9
  13.8 3.0 fusion.11
  19.5 37.0 %all-gather.7.cloned.1.call-done = bf16[3,2048,128]{2,1,0:T(8,128)(2,1)} async-done(((bf16[3,256,128]{2,1,0:T(8,128)(2,1)}), bf16[3,2048,128]{2,1,0:T(8,128)(2,1)}) %all-gather.7.cloned.1.call-update) | async-done | bytes 1572880 | tf_op jit(solution)/shard_map/all_gather | solution.py:83
  56.5 3.8 convolution_multiply_fusion.5
  60.4 40.8 %all-gather.9.cloned.1.call-done = bf16[3,2048,128]{2,1,0:T(8,128)(2,1)} async-done(((bf16[3,256,128]{2,1,0:T(8,128)(2,1)}), bf16[3,2048,128]{2,1,0:T(8,128)(2,1)}) %all-gather.9.cloned.1.call-update) | async-done | bytes 1572880 | tf_op jit(solution)/shard_map/all_gather | solution.py:84
  101.3 3.8 convolution_convert_fusion.3
  106.4 5.0 collective-permute-start
  114.4 48.1 %all-gather.11.cloned.1.call-done = bf16[3,2048,256]{2,1,0:T(8,128)(2,1)} async-done(((bf16[3,256,256]{2,1,0:T(8,128)(2,1)}), bf16[3,2048,256]{2,1,0:T(8,128)(2,1)}) %all-gather.11.cloned.1.call-update) | async-done | bytes 3145744 | tf_op jit(solution)/shard_map/all_gather | solution.py:82
  162.4 3.8 convolution_multiply_fusion.2
  166.4 3.7 fusion.3
  170.2 4.7 fusion
  174.9 6.2 %fusion.24 = bf16[2,64,2,1024]{3,1,2,0:T(8,128)(2,1)S(1)} fusion(bf16[1280,2,64,1]{0,2,3,1:T(8,128)(2,1)S(1)} %bitcast.159, f32[2,1280,1024,2]{2,1,3,0:T(8,128)S(1)} %get-tuple-element.38, f32[2,2,1024]{2,1,0:T(2,128)S(1)} %exponential_add_fusion.2, f32[2,2,1024]{2,1,0:T(2,128)S(1)} %broadcast_maximum_fusion.2, pred[1024,1280]{0,1:T(8,128)(4,1)S(1)} %fusion.19), kind=kOutput, calls=%fused_computation.46 | convolution fusion | flops 697565184 | bytes 23166976 | tf_op jit(solution)/shard_map/kgqs,skd->qkgd/dot_general | solution.py:59
  181.1 42.1 %all-gather.13.cloned.1.call-done = bf16[3,2048,256]{2,1,0:T(8,128)(2,1)} async-done(((bf16[3,256,256]{2,1,0:T(8,128)(2,1)}), bf16[3,2048,256]{2,1,0:T(8,128)(2,1)}) %all-gather.13.cloned.1.call-update) | async-done | bytes 3145744 | tf_op jit(solution)/shard_map/all_gather | solution.py:85
  223.2 5.8 fusion.26
  229.1 70.2 %reduce-scatter.4.cloned.1.call-done = f32[256,2048]{1,0:T(8,128)} async-done(((f32[1024,2048]{1,0:T(8,128)}), f32[256,2048]{1,0:T(8,128)}) %reduce-scatter.4.cloned.1.call-update) | async-done | bytes 2097168 | tf_op jit(solution)/shard_map/reduce_scatter | solution.py:123
  302.3 34.3 %all-gather.15.cloned.1.call-done = bf16[1024,2048]{1,0:T(8,128)(2,1)} async-done(((bf16[256,2048]{1,0:T(8,128)(2,1)}), bf16[1024,2048]{1,0:T(8,128)(2,1)}) %all-gather.15.cloned.1.call-update) | async-done | bytes 4194320 | tf_op jit(solution)/shard_map/all_gather | solution.py:126
  336.6 3.2 fusion.12
  346.8 4.5 collective-permute-start.2
  354.9 3.7 fusion.4
  358.7 4.7 fusion.1
  363.4 7.8 %fusion.23 = bf16[2,64,2,1024]{3,1,2,0:T(8,128)(2,1)} fusion(bf16[1280,2,64,1]{0,2,3,1:T(8,128)(2,1)} %bitcast.161, f32[2,1280,1024,2]{2,1,3,0:T(8,128)S(1)} %get-tuple-element.40, f32[2,2,1024]{2,1,0:T(2,128)S(1)} %exponential_add_fusion.1, f32[2,2,1024]{2,1,0:T(2,128)S(1)} %broadcast_maximum_fusion.1, pred[1024,1280]{0,1:T(8,128)(4,1)S(1)} %fusion.19), kind=kOutput, calls=%fused_computation.45 | convolution fusion | flops 697565184 | bytes 23166976 | tf_op jit(solution)/shard_map/kgqs,skd->qkgd/dot_general | solution.py:59
  371.2 5.9 %fusion.25 = f32[1024,2048]{1,0:T(8,128)} fusion(bf16[1024,256]{0,1:T(8,128)(2,1)} %bitcast.158, bf16[3,2048,256]{2,1,0:T(8,128)(2,1)} %all-gather.13.cloned.1.call-done), kind=kOutput, calls=%fused_computation.56 | convolution fusion | flops 1073741824 | bytes 9961472 | tf_op jit(solution)/shard_map/dot_general | solution.py:118
  377.2 72.4 %reduce-scatter.6.cloned.1.call-done = f32[256,2048]{1,0:T(8,128)} async-done(((f32[1024,2048]{1,0:T(8,128)}), f32[256,2048]{1,0:T(8,128)}) %reduce-scatter.6.cloned.1.call-update) | async-done | bytes 2097168 | tf_op jit(solution)/shard_map/reduce_scatter | solution.py:123
  452.7 34.3 %all-gather.17.cloned.1.call-done = bf16[1024,2048]{1,0:T(8,128)(2,1)} async-done(((bf16[256,2048]{1,0:T(8,128)(2,1)}), bf16[1024,2048]{1,0:T(8,128)(2,1)}) %all-gather.17.cloned.1.call-update) | async-done | bytes 4194320 | tf_op jit(solution)/shard_map/all_gather | solution.py:126
  487.0 3.2 fusion.15
  497.0 4.5 collective-permute-start.4
  504.5 3.7 fusion.5
  508.2 4.7 fusion.2
  513.0 6.2 %fusion.22 = bf16[2,64,2,1024]{3,1,2,0:T(8,128)(2,1)S(1)} fusion(bf16[1280,2,64,1]{0,2,3,1:T(8,128)(2,1)S(1)} %bitcast.160, f32[2,1280,1024,2]{2,1,3,0:T(8,128)S(1)} %get-tuple-element.42, f32[2,2,1024]{2,1,0:T(2,128)S(1)} %exponential_add_fusion, f32[2,2,1024]{2,1,0:T(2,128)S(1)} %broadcast_maximum_fusion, pred[1024,1280]{0,1:T(8,128)(4,1)S(1)} %fusion.19), kind=kOutput, calls=%fused_computation.44 | convolution fusion | flops 697565184 | bytes 23166976 | tf_op jit(solution)/shard_map/kgqs,skd->qkgd/dot_general | solution.py:59
  519.2 4.5 convolution_convert_fusion
  523.7 45.7 %reduce-scatter.8.cloned.1.call-done = bf16[256,2048]{1,0:T(8,128)(2,1)} async-done(((bf16[1024,2048]{1,0:T(8,128)(2,1)}), bf16[256,2048]{1,0:T(8,128)(2,1)}) %reduce-scatter.8.cloned.1.call-update) | async-done | bytes 1048592 | tf_op jit(solution)/shard_map/reduce_scatter | solution.py:128
  570.9 2.8 fusion.21
  (89 shorter events, 39.2 us)
Async XLA Ops:
  6.5 50.0 %all-gather.7.cloned.1.call-start = ((), (), s32[]{:S(2)}) async-start(), calls=%async_computation.3 | async-start | bytes 1769472 | tf_op jit(solution)/shard_map/all_gather | solution.py:83
  7.3 94.0 %all-gather.9.cloned.1.call-start = ((), (), s32[]{:S(2)}) async-start(), calls=%async_computation.4 | async-start | bytes 1769472 | tf_op jit(solution)/shard_map/all_gather | solution.py:84
  8.0 154.4 %all-gather.11.cloned.1.call-start = ((), (), s32[]{:S(2)}) async-start(), calls=%async_computation.5 | async-start | bytes 3538944 | tf_op jit(solution)/shard_map/all_gather | solution.py:82
  8.7 214.5 %all-gather.13.cloned.1.call-start = ((), (), s32[]{:S(2)}) async-start(), calls=%async_computation.6 | async-start | bytes 3538944 | tf_op jit(solution)/shard_map/all_gather | solution.py:85
  9.3 289.9 %reduce-scatter.4.cloned.1.call-start = ((), (), s32[]{:S(2)}) async-start(), calls=%async_computation.7 | async-start | bytes 10485760 | tf_op jit(solution)/shard_map/reduce_scatter | solution.py:123
  9.4 4.4 copy-start
  19.5 91.9 %copy-start.5 = (f32[3,4]{1,0:T(4,128)S(1)}, f32[3,4]{1,0:T(4,128)}, u32[]{:S(2)}) copy-start(f32[3,4]{1,0:T(4,128)} %param.14) | copy-start | bytes 148
  105.1 6.4 %collective-permute-start.1 = (bf16[128,256]{0,1:T(8,128)(2,1)S(1)}, bf16[128,256]{0,1:T(8,128)(2,1)S(1)}, u32[]{:S(2)}, u32[]{:S(2)}) collective-permute-start(bf16[128,256]{0,1:T(8,128)(2,1)S(1)} %get-tuple-element.31), channel_id=1, source_target_pairs={{4,0},{8,4},{12,8},{16,12},{20,16},{24,20},{28,24},{5,1},{9,5},{13... | collective-permute-start | bytes 196616 | tf_op jit(solution)/shard_map/ppermute | solution.py:21
  106.4 7.8 %collective-permute-start = (bf16[128,256]{0,1:T(8,128)(2,1)S(1)}, bf16[128,256]{0,1:T(8,128)(2,1)S(1)}, u32[]{:S(2)}, u32[]{:S(2)}) collective-permute-start(bf16[128,256]{0,1:T(8,128)(2,1)S(1)} %get-tuple-element.30), channel_id=1, source_target_pairs={{0,4},{4,8},{8,12},{12,16},{16,20},{20,24},{24,28},{1,5},{5,9},{9,... | collective-permute-start | bytes 196616 | tf_op jit(solution)/shard_map/ppermute | solution.py:18
  229.0 107.6 %all-gather.15.cloned.1.call-start = ((), (), s32[]{:S(2)}) async-start(), calls=%async_computation.8 | async-start | bytes 5242880 | tf_op jit(solution)/shard_map/all_gather | solution.py:126
  302.0 147.7 %reduce-scatter.6.cloned.1.call-start = ((), (), s32[]{:S(2)}) async-start(), calls=%async_computation.9 | async-start | bytes 10485760 | tf_op jit(solution)/shard_map/reduce_scatter | solution.py:123
  336.6 3.4 copy-start.2
  341.1 2.8 copy-start.3
  345.5 8.6 %collective-permute-start.3 = (bf16[128,256]{0,1:T(8,128)(2,1)S(1)}, bf16[128,256]{0,1:T(8,128)(2,1)S(1)}, u32[]{:S(2)}, u32[]{:S(2)}) collective-permute-start(bf16[128,256]{0,1:T(8,128)(2,1)S(1)} %get-tuple-element.29), channel_id=1, source_target_pairs={{4,0},{8,4},{12,8},{16,12},{20,16},{24,20},{28,24},{5,1},{9,5},{13... | collective-permute-start | bytes 196616 | tf_op jit(solution)/shard_map/ppermute | solution.py:21
  346.8 7.3 %collective-permute-start.2 = (bf16[128,256]{0,1:T(8,128)(2,1)S(1)}, bf16[128,256]{0,1:T(8,128)(2,1)S(1)}, u32[]{:S(2)}, u32[]{:S(2)}) collective-permute-start(bf16[128,256]{0,1:T(8,128)(2,1)S(1)} %get-tuple-element.28), channel_id=1, source_target_pairs={{0,4},{4,8},{8,12},{12,16},{16,20},{20,24},{24,28},{1,5},{5,9},{9,... | collective-permute-start | bytes 196616 | tf_op jit(solution)/shard_map/ppermute | solution.py:18
  377.2 109.8 %all-gather.17.cloned.1.call-start = ((), (), s32[]{:S(2)}) async-start(), calls=%async_computation.10 | async-start | bytes 5242880 | tf_op jit(solution)/shard_map/all_gather | solution.py:126
  452.4 117.0 %reduce-scatter.8.cloned.1.call-start = ((), (), s32[]{:S(2)}) async-start(), calls=%async_computation.11 | async-start | bytes 5242880 | tf_op jit(solution)/shard_map/reduce_scatter | solution.py:128
  487.0 3.4 copy-start.1
  495.7 8.6 %collective-permute-start.5 = (bf16[128,256]{0,1:T(8,128)(2,1)S(1)}, bf16[128,256]{0,1:T(8,128)(2,1)S(1)}, u32[]{:S(2)}, u32[]{:S(2)}) collective-permute-start(bf16[128,256]{0,1:T(8,128)(2,1)S(1)} %get-tuple-element.27), channel_id=1, source_target_pairs={{4,0},{8,4},{12,8},{16,12},{20,16},{24,20},{28,24},{5,1},{9,5},{13... | collective-permute-start | bytes 196616 | tf_op jit(solution)/shard_map/ppermute | solution.py:21
  497.0 7.3 %collective-permute-start.4 = (bf16[128,256]{0,1:T(8,128)(2,1)S(1)}, bf16[128,256]{0,1:T(8,128)(2,1)S(1)}, u32[]{:S(2)}, u32[]{:S(2)}) collective-permute-start(bf16[128,256]{0,1:T(8,128)(2,1)S(1)} %get-tuple-element.26), channel_id=1, source_target_pairs={{0,4},{4,8},{8,12},{12,16},{16,20},{20,24},{24,28},{1,5},{5,9},{9,... | collective-permute-start | bytes 196616 | tf_op jit(solution)/shard_map/ppermute | solution.py:18
  519.2 51.7 %copy-start.4 = (f32[2048]{0:T(1024)S(1)}, f32[2048]{0:T(1024)}, u32[]{:S(2)}) copy-start(f32[2048]{0:T(1024)} %param.15) | copy-start | bytes 24580
Sparse Core Ops, SparseCore 0:
  9.5 46.9 all-gather.6
  58.7 42.5 all-gather.8
  103.5 58.9 all-gather.10
  164.5 58.7 all-gather.12
  229.2 70.0 reduce-scatter.3
  302.1 34.4 all-gather.14
  377.3 72.3 reduce-scatter.5
  452.5 34.4 all-gather.16
  523.9 45.4 reduce-scatter.7
where the time goes:
time: 586 us; the launch traced here: 581 us
  waiting for transfers between devices  430 us (73%)
  matrix products  72.3 us (12%)
  other arithmetic  42.9 us (7%)
  starting transfers between devices  18.7 us (3%)
  between operations  13.9 us (2%)
    reduce_scatter x2, waiting for transfers between devices, shards(): lax.psum_scatter(project(), 'tp', scatter_dimension=0, tiled=True)  143 us
    all_gather x2, waiting for transfers between devices, shards(): current = lax.all_gather(share_rows, 'tp', axis=0, tiled=True)  68.6 us
    all_gather x1, waiting for transfers between devices, shards(): lax.all_gather(query_weight, 'sp', axis=1, tiled=True)  48.1 us
    reduce_scatter x1, waiting for transfers between devices, shards(): lax.psum_scatter(project().astype(jnp.bfloat16), 'tp', scatter_dimension=...  45.7 us
    all_gather x1, waiting for transfers between devices, shards(): lax.all_gather(output_weight, 'sp', axis=1, tiled=True)  42.1 us
    all_gather x1, waiting for transfers between devices, shards(): lax.all_gather(value_weight, 'sp', axis=1, tiled=True)  40.8 us
    all_gather x1, waiting for transfers between devices, shards(): lax.all_gather(key_weight, 'sp', axis=1, tiled=True)  37 us
    dot_general x3, matrix products, attend(): jnp.einsum('kgqs,skd->qkgd', weights, value_rows, preferred_element_type=...  20.2 us
  transfers between devices with their start and end apart: 15, of which 10 were waited for; matrix products, arithmetic and copies ran while one was open for 7% of the time, Pallas kernels for 0%

commit v1 on v0

--- a/solution.py
+++ b/solution.py
@@ -123,7 +123,15 @@
             share_rows = lax.psum_scatter(project(), "tp", scatter_dimension=0, tiled=True).astype(
                 jnp.bfloat16
             )
-            current = lax.all_gather(share_rows, "tp", axis=0, tiled=True)
+            devices = lax.axis_size("tp")
+            held, blocks = (share_rows, [share_rows])
+            for _ in range(devices - 1):
+                held = lax.ppermute(
+                    held, "tp", [(i_2, (i_2 + 1) % devices) for i_2 in range(devices)]
+                )
+                blocks.insert(0, held)
+            line = jnp.concatenate(blocks, axis=0)
+            current = jnp.roll(line, (lax.axis_index("tp") + 1) * share_rows.shape[0], axis=0)
         else:
             final_rows = lax.psum_scatter(
                 project().astype(jnp.bfloat16), "tp", scatter_dimension=0, tiled=True

time: 586 us -> 613 us (1.046)
  waiting for transfers between devices: 430 us -> 446 us
  other arithmetic: 42.9 us -> 53.4 us
    ppermute x0 -> x6, waiting for transfers between devices: none -> 85.9 us  [shards(): lax.ppermute(held, 'tp', [(i_2, (i_2 + 1) % devices) for i_2 in range(dev...]
    all_gather x2 -> x0, waiting for transfers between devices: 68.6 us -> none  [shards(): current = lax.all_gather(share_rows, 'tp', axis=0, tiled=True)]
    reduce_sum x4, other arithmetic: 11.3 us -> 21.6 us  [norm_rows(): jnp.mean(wide_values * wide_values, axis=-1, keepdims=True) + EPS]
  transfers between devices with their start and end apart: 15 -> 19, of which waited for: 10 -> 14; matrix products, arithmetic and copies ran while one was open for 7% -> 7% of each run, Pallas kernels for 0% -> 0%
where the time goes in v1:
time: 613 us; the launch traced here: 608 us
  waiting for transfers between devices  446 us (73%)
  matrix products  72.5 us (12%)
  other arithmetic  53.4 us (9%)
  starting transfers between devices  18.7 us (3%)
  between operations  14.3 us (2%)
    reduce_scatter x2, waiting for transfers between devices, shards(): lax.psum_scatter(project(), 'tp', scatter_dimension=0, tiled=True)  143 us
    ppermute x6, waiting for transfers between devices, shards(): lax.ppermute(held, 'tp', [(i_2, (i_2 + 1) % devices) for i_2 in range(dev...  85.9 us
    all_gather x1, waiting for transfers between devices, shards(): lax.all_gather(query_weight, 'sp', axis=1, tiled=True)  48.1 us
    reduce_scatter x1, waiting for transfers between devices, shards(): lax.psum_scatter(project().astype(jnp.bfloat16), 'tp', scatter_dimension=...  45.7 us
    all_gather x1, waiting for transfers between devices, shards(): lax.all_gather(output_weight, 'sp', axis=1, tiled=True)  42.1 us
    all_gather x1, waiting for transfers between devices, shards(): lax.all_gather(value_weight, 'sp', axis=1, tiled=True)  40.8 us
    all_gather x1, waiting for transfers between devices, shards(): lax.all_gather(key_weight, 'sp', axis=1, tiled=True)  35.1 us
    reduce_sum x4, other arithmetic, norm_rows(): jnp.mean(wide_values * wide_values, axis=-1, keepdims=True) + EPS  21.6 us
  transfers between devices with their start and end apart: 19, of which 14 were waited for; matrix products, arithmetic and copies ran while one was open for 7% of the time, Pallas kernels for 0%

profile of v1, /device:TPU:0, one launch (start us, length us, event | category | flops | bytes accessed | tf_op | source)
XLA Modules:
  0.0 607.8 jit_solution(10370509634117768333)
XLA Ops:
  13.4 5.2 fusion.11
  21.4 35.1 %all-gather.5.cloned.1.call-done = bf16[3,2048,128]{2,1,0:T(8,128)(2,1)} async-done(((bf16[3,256,128]{2,1,0:T(8,128)(2,1)}), bf16[3,2048,128]{2,1,0:T(8,128)(2,1)}) %all-gather.5.cloned.1.call-update) | async-done | bytes 1572880 | tf_op jit(solution)/shard_map/all_gather | solution.py:83
  56.5 3.8 convolution_multiply_fusion.5
  60.4 40.8 %all-gather.7.cloned.1.call-done = bf16[3,2048,128]{2,1,0:T(8,128)(2,1)} async-done(((bf16[3,256,128]{2,1,0:T(8,128)(2,1)}), bf16[3,2048,128]{2,1,0:T(8,128)(2,1)}) %all-gather.7.cloned.1.call-update) | async-done | bytes 1572880 | tf_op jit(solution)/shard_map/all_gather | solution.py:84
  101.2 3.8 convolution_convert_fusion.3
  106.4 5.0 collective-permute-start
  114.3 48.1 %all-gather.9.cloned.1.call-done = bf16[3,2048,256]{2,1,0:T(8,128)(2,1)} async-done(((bf16[3,256,256]{2,1,0:T(8,128)(2,1)}), bf16[3,2048,256]{2,1,0:T(8,128)(2,1)}) %all-gather.9.cloned.1.call-update) | async-done | bytes 3145744 | tf_op jit(solution)/shard_map/all_gather | solution.py:82
  162.4 3.8 convolution_multiply_fusion.2
  170.1 4.7 fusion
  174.9 6.2 %fusion.38 = bf16[2,64,2,1024]{3,1,2,0:T(8,128)(2,1)S(1)} fusion(bf16[1280,2,64,1]{0,2,3,1:T(8,128)(2,1)S(1)} %bitcast.159, f32[2,1280,1024,2]{2,1,3,0:T(8,128)S(1)} %get-tuple-element.43, f32[2,2,1024]{2,1,0:T(2,128)S(1)} %exponential_add_fusion.2, f32[2,2,1024]{2,1,0:T(2,128)S(1)} %broadcast_maximum_fusion.2, pred[1024,1280]{0,1:T(8,128)(4,1)S(1)} %fusion.19), kind=kOutput, calls=%fused_computation.76 | convolution fusion | flops 697565184 | bytes 23166976 | tf_op jit(solution)/shard_map/kgqs,skd->qkgd/dot_general | solution.py:59
  181.1 42.1 %all-gather.11.cloned.1.call-done = bf16[3,2048,256]{2,1,0:T(8,128)(2,1)} async-done(((bf16[3,256,256]{2,1,0:T(8,128)(2,1)}), bf16[3,2048,256]{2,1,0:T(8,128)(2,1)}) %all-gather.11.cloned.1.call-update) | async-done | bytes 3145744 | tf_op jit(solution)/shard_map/all_gather | solution.py:85
  223.2 5.8 fusion.40
  229.0 70.2 %reduce-scatter.4.cloned.1.call-done = f32[256,2048]{1,0:T(8,128)} async-done(((f32[1024,2048]{1,0:T(8,128)}), f32[256,2048]{1,0:T(8,128)}) %reduce-scatter.4.cloned.1.call-update) | async-done | bytes 2097168 | tf_op jit(solution)/shard_map/reduce_scatter | solution.py:123
  301.0 14.2 %collective-permute-done.2 = bf16[256,2048]{1,0:T(8,128)(2,1)S(1)} collective-permute-done((bf16[256,2048]{1,0:T(8,128)(2,1)S(1)}, bf16[256,2048]{1,0:T(8,128)(2,1)S(1)}, u32[]{:S(2)}, u32[]{:S(2)}) %collective-permute-start.2) | collective-permute-done | bytes 1048608 | tf_op jit(solution)/shard_map/ppermute | solution.py:129
  316.2 14.3 %collective-permute-done.3 = bf16[256,2048]{1,0:T(8,128)(2,1)} collective-permute-done((bf16[256,2048]{1,0:T(8,128)(2,1)S(1)}, bf16[256,2048]{1,0:T(8,128)(2,1)}, u32[]{:S(2)}, u32[]{:S(2)}) %collective-permute-start.3) | collective-permute-done | bytes 1048608 | tf_op jit(solution)/shard_map/ppermute | solution.py:129
  330.8 14.4 %collective-permute-done.4 = bf16[256,2048]{1,0:T(8,128)(2,1)} collective-permute-done((bf16[256,2048]{1,0:T(8,128)(2,1)}, bf16[256,2048]{1,0:T(8,128)(2,1)}, u32[]{:S(2)}, u32[]{:S(2)}) %collective-permute-start.4) | collective-permute-done | bytes 1048608 | tf_op jit(solution)/shard_map/ppermute | solution.py:129
  345.2 8.5 %fusion.12 = (f32[1024]{0:T(1024)S(1)}, bf16[1024,2048]{1,0:T(8,128)(2,1)S(1)}) fusion(s32[]{:T(128)S(6)} %select_n.26, bf16[256,2048]{1,0:T(8,128)(2,1)S(1)} %convert_element_type.115, bf16[256,2048]{1,0:T(8,128)(2,1)} %copy-done, bf16[256,2048]{1,0:T(8,128)(2,1)} %collective-permute-done.3, bf16[256,2048]{1,0:T(8,128)(2,1)} %collective-permute-done.4), kind=kLoop, calls=%fused_computation.27 | loop fusion | flops 39844864 | bytes 8392708 | tf_op jit(solution)/shard_map/reduce_sum | solution.py:28
  361.3 4.5 collective-permute-start.5
  368.8 3.7 fusion.4
  372.5 4.7 fusion.1
  377.3 6.2 %fusion.37 = bf16[2,64,2,1024]{3,1,2,0:T(8,128)(2,1)S(1)} fusion(bf16[1280,2,64,1]{0,2,3,1:T(8,128)(2,1)S(1)} %bitcast.161, f32[2,1280,1024,2]{2,1,3,0:T(8,128)S(1)} %get-tuple-element.45, f32[2,2,1024]{2,1,0:T(2,128)S(1)} %exponential_add_fusion.1, f32[2,2,1024]{2,1,0:T(2,128)S(1)} %broadcast_maximum_fusion.1, pred[1024,1280]{0,1:T(8,128)(4,1)S(1)} %fusion.19), kind=kOutput, calls=%fused_computation.75 | convolution fusion | flops 697565184 | bytes 23166976 | tf_op jit(solution)/shard_map/kgqs,skd->qkgd/dot_general | solution.py:59
  383.5 5.8 fusion.39
  389.4 72.4 %reduce-scatter.6.cloned.1.call-done = f32[256,2048]{1,0:T(8,128)} async-done(((f32[1024,2048]{1,0:T(8,128)}), f32[256,2048]{1,0:T(8,128)}) %reduce-scatter.6.cloned.1.call-update) | async-done | bytes 2097168 | tf_op jit(solution)/shard_map/reduce_scatter | solution.py:123
  463.6 14.2 %collective-permute-done.7 = bf16[256,2048]{1,0:T(8,128)(2,1)S(1)} collective-permute-done((bf16[256,2048]{1,0:T(8,128)(2,1)S(1)}, bf16[256,2048]{1,0:T(8,128)(2,1)S(1)}, u32[]{:S(2)}, u32[]{:S(2)}) %collective-permute-start.7) | collective-permute-done | bytes 1048608 | tf_op jit(solution)/shard_map/ppermute | solution.py:129
  478.8 14.3 %collective-permute-done.8 = bf16[256,2048]{1,0:T(8,128)(2,1)} collective-permute-done((bf16[256,2048]{1,0:T(8,128)(2,1)S(1)}, bf16[256,2048]{1,0:T(8,128)(2,1)}, u32[]{:S(2)}, u32[]{:S(2)}) %collective-permute-start.8) | collective-permute-done | bytes 1048608 | tf_op jit(solution)/shard_map/ppermute | solution.py:129
  493.4 14.4 %collective-permute-done.9 = bf16[256,2048]{1,0:T(8,128)(2,1)} collective-permute-done((bf16[256,2048]{1,0:T(8,128)(2,1)}, bf16[256,2048]{1,0:T(8,128)(2,1)}, u32[]{:S(2)}, u32[]{:S(2)}) %collective-permute-start.9) | collective-permute-done | bytes 1048608 | tf_op jit(solution)/shard_map/ppermute | solution.py:129
  507.8 8.5 %fusion.15 = (f32[1024]{0:T(1024)S(1)}, bf16[1024,2048]{1,0:T(8,128)(2,1)S(1)}) fusion(s32[]{:T(128)S(6)} %select_n.26, bf16[256,2048]{1,0:T(8,128)(2,1)S(1)} %convert_element_type.123, bf16[256,2048]{1,0:T(8,128)(2,1)} %copy-done.1, bf16[256,2048]{1,0:T(8,128)(2,1)} %collective-permute-done.8, bf16[256,2048]{1,0:T(8,128)(2,1)} %collective-permute-done.9), kind=kLoop, calls=%fused_computation.30 | loop fusion | flops 39844864 | bytes 8392708 | tf_op jit(solution)/shard_map/reduce_sum | solution.py:28
  524.0 4.5 collective-permute-start.10
  535.2 4.7 fusion.2
  540.0 6.2 %fusion.36 = bf16[2,64,2,1024]{3,1,2,0:T(8,128)(2,1)S(1)} fusion(bf16[1280,2,64,1]{0,2,3,1:T(8,128)(2,1)S(1)} %bitcast.160, f32[2,1280,1024,2]{2,1,3,0:T(8,128)S(1)} %get-tuple-element.47, f32[2,2,1024]{2,1,0:T(2,128)S(1)} %exponential_add_fusion, f32[2,2,1024]{2,1,0:T(2,128)S(1)} %broadcast_maximum_fusion, pred[1024,1280]{0,1:T(8,128)(4,1)S(1)} %fusion.19), kind=kOutput, calls=%fused_computation.74 | convolution fusion | flops 697565184 | bytes 23166976 | tf_op jit(solution)/shard_map/kgqs,skd->qkgd/dot_general | solution.py:59
  546.2 4.5 convolution_convert_fusion
  550.7 45.7 %reduce-scatter.8.cloned.1.call-done = bf16[256,2048]{1,0:T(8,128)(2,1)} async-done(((bf16[1024,2048]{1,0:T(8,128)(2,1)}), bf16[256,2048]{1,0:T(8,128)(2,1)}) %reduce-scatter.8.cloned.1.call-update) | async-done | bytes 1048592 | tf_op jit(solution)/shard_map/reduce_scatter | solution.py:136
  (91 shorter events, 53.1 us)
Async XLA Ops:
  6.5 49.9 %all-gather.5.cloned.1.call-start = ((), (), s32[]{:S(2)}) async-start(), calls=%async_computation.3 | async-start | bytes 1769472 | tf_op jit(solution)/shard_map/all_gather | solution.py:83
  7.3 94.0 %all-gather.7.cloned.1.call-start = ((), (), s32[]{:S(2)}) async-start(), calls=%async_computation.4 | async-start | bytes 1769472 | tf_op jit(solution)/shard_map/all_gather | solution.py:84
  8.0 154.4 %all-gather.9.cloned.1.call-start = ((), (), s32[]{:S(2)}) async-start(), calls=%async_computation.5 | async-start | bytes 3538944 | tf_op jit(solution)/shard_map/all_gather | solution.py:82
  8.7 214.5 %all-gather.11.cloned.1.call-start = ((), (), s32[]{:S(2)}) async-start(), calls=%async_computation.6 | async-start | bytes 3538944 | tf_op jit(solution)/shard_map/all_gather | solution.py:85
  9.3 289.9 %reduce-scatter.4.cloned.1.call-start = ((), (), s32[]{:S(2)}) async-start(), calls=%async_computation.7 | async-start | bytes 10485760 | tf_op jit(solution)/shard_map/reduce_scatter | solution.py:123
  18.6 92.8 %copy-start.3 = (f32[3,4]{1,0:T(4,128)S(1)}, f32[3,4]{1,0:T(4,128)}, u32[]{:S(2)}) copy-start(f32[3,4]{1,0:T(4,128)} %param.16) | copy-start | bytes 148
  105.1 6.4 %collective-permute-start.1 = (bf16[128,256]{0,1:T(8,128)(2,1)S(1)}, bf16[128,256]{0,1:T(8,128)(2,1)S(1)}, u32[]{:S(2)}, u32[]{:S(2)}) collective-permute-start(bf16[128,256]{0,1:T(8,128)(2,1)S(1)} %get-tuple-element.36), channel_id=1, source_target_pairs={{4,0},{8,4},{12,8},{16,12},{20,16},{24,20},{28,24},{5,1},{9,5},{13... | collective-permute-start | bytes 196616 | tf_op jit(solution)/shard_map/ppermute | solution.py:21
  106.4 7.8 %collective-permute-start = (bf16[128,256]{0,1:T(8,128)(2,1)S(1)}, bf16[128,256]{0,1:T(8,128)(2,1)S(1)}, u32[]{:S(2)}, u32[]{:S(2)}) collective-permute-start(bf16[128,256]{0,1:T(8,128)(2,1)S(1)} %get-tuple-element.35), channel_id=1, source_target_pairs={{0,4},{4,8},{8,12},{12,16},{16,20},{20,24},{24,28},{1,5},{5,9},{9,... | collective-permute-start | bytes 196616 | tf_op jit(solution)/shard_map/ppermute | solution.py:18
  229.0 232.8 %reduce-scatter.6.cloned.1.call-start = ((), (), s32[]{:S(2)}) async-start(), calls=%async_computation.8 | async-start | bytes 10485760 | tf_op jit(solution)/shard_map/reduce_scatter | solution.py:123
  300.9 14.3 %collective-permute-start.2 = (bf16[256,2048]{1,0:T(8,128)(2,1)S(1)}, bf16[256,2048]{1,0:T(8,128)(2,1)S(1)}, u32[]{:S(2)}, u32[]{:S(2)}) collective-permute-start(bf16[256,2048]{1,0:T(8,128)(2,1)S(1)} %convert_element_type.115), channel_id=1, source_target_pairs={{0,1},{1,2},{2,3},{3,0},{4,5},{5,6},{6,7},{7,4},{8,9},{9,10},{10,1... | collective-permute-start | bytes 3145736 | tf_op jit(solution)/shard_map/ppermute | solution.py:129
  315.2 1.0 copy-start
  316.2 14.3 %collective-permute-start.3 = (bf16[256,2048]{1,0:T(8,128)(2,1)S(1)}, bf16[256,2048]{1,0:T(8,128)(2,1)}, u32[]{:S(2)}, u32[]{:S(2)}) collective-permute-start(bf16[256,2048]{1,0:T(8,128)(2,1)S(1)} %collective-permute-done.2), channel_id=1, source_target_pairs={{0,1},{1,2},{2,3},{3,0},{4,5},{5,6},{6,7},{7,4},{8,9},{9,10},{10,1... | collective-permute-start | bytes 3145736 | tf_op jit(solution)/shard_map/ppermute | solution.py:129
  330.5 14.7 %collective-permute-start.4 = (bf16[256,2048]{1,0:T(8,128)(2,1)}, bf16[256,2048]{1,0:T(8,128)(2,1)}, u32[]{:S(2)}, u32[]{:S(2)}) collective-permute-start(bf16[256,2048]{1,0:T(8,128)(2,1)} %collective-permute-done.3), channel_id=1, source_target_pairs={{0,1},{1,2},{2,3},{3,0},{4,5},{5,6},{6,7},{7,4},{8,9},{9,10},{10,1... | collective-permute-start | bytes 3145736 | tf_op jit(solution)/shard_map/ppermute | solution.py:129
  360.0 8.6 %collective-permute-start.6 = (bf16[128,256]{0,1:T(8,128)(2,1)S(1)}, bf16[128,256]{0,1:T(8,128)(2,1)S(1)}, u32[]{:S(2)}, u32[]{:S(2)}) collective-permute-start(bf16[128,256]{0,1:T(8,128)(2,1)S(1)} %get-tuple-element.34), channel_id=1, source_target_pairs={{4,0},{8,4},{12,8},{16,12},{20,16},{24,20},{28,24},{5,1},{9,5},{13... | collective-permute-start | bytes 196616 | tf_op jit(solution)/shard_map/ppermute | solution.py:21
  361.3 7.3 %collective-permute-start.5 = (bf16[128,256]{0,1:T(8,128)(2,1)S(1)}, bf16[128,256]{0,1:T(8,128)(2,1)S(1)}, u32[]{:S(2)}, u32[]{:S(2)}) collective-permute-start(bf16[128,256]{0,1:T(8,128)(2,1)S(1)} %get-tuple-element.33), channel_id=1, source_target_pairs={{0,4},{4,8},{8,12},{12,16},{16,20},{20,24},{24,28},{1,5},{5,9},{9,... | collective-permute-start | bytes 196616 | tf_op jit(solution)/shard_map/ppermute | solution.py:18
  389.3 207.1 %reduce-scatter.8.cloned.1.call-start = ((), (), s32[]{:S(2)}) async-start(), calls=%async_computation.9 | async-start | bytes 5242880 | tf_op jit(solution)/shard_map/reduce_scatter | solution.py:136
  463.5 14.3 %collective-permute-start.7 = (bf16[256,2048]{1,0:T(8,128)(2,1)S(1)}, bf16[256,2048]{1,0:T(8,128)(2,1)S(1)}, u32[]{:S(2)}, u32[]{:S(2)}) collective-permute-start(bf16[256,2048]{1,0:T(8,128)(2,1)S(1)} %convert_element_type.123), channel_id=1, source_target_pairs={{0,1},{1,2},{2,3},{3,0},{4,5},{5,6},{6,7},{7,4},{8,9},{9,10},{10,1... | collective-permute-start | bytes 3145736 | tf_op jit(solution)/shard_map/ppermute | solution.py:129
  477.8 1.0 copy-start.1
  478.8 14.3 %collective-permute-start.8 = (bf16[256,2048]{1,0:T(8,128)(2,1)S(1)}, bf16[256,2048]{1,0:T(8,128)(2,1)}, u32[]{:S(2)}, u32[]{:S(2)}) collective-permute-start(bf16[256,2048]{1,0:T(8,128)(2,1)S(1)} %collective-permute-done.7), channel_id=1, source_target_pairs={{0,1},{1,2},{2,3},{3,0},{4,5},{5,6},{6,7},{7,4},{8,9},{9,10},{10,1... | collective-permute-start | bytes 3145736 | tf_op jit(solution)/shard_map/ppermute | solution.py:129
  493.1 14.7 %collective-permute-start.9 = (bf16[256,2048]{1,0:T(8,128)(2,1)}, bf16[256,2048]{1,0:T(8,128)(2,1)}, u32[]{:S(2)}, u32[]{:S(2)}) collective-permute-start(bf16[256,2048]{1,0:T(8,128)(2,1)} %collective-permute-done.8), channel_id=1, source_target_pairs={{0,1},{1,2},{2,3},{3,0},{4,5},{5,6},{6,7},{7,4},{8,9},{9,10},{10,1... | collective-permute-start | bytes 3145736 | tf_op jit(solution)/shard_map/ppermute | solution.py:129
  522.7 8.6 %collective-permute-start.11 = (bf16[128,256]{0,1:T(8,128)(2,1)S(1)}, bf16[128,256]{0,1:T(8,128)(2,1)S(1)}, u32[]{:S(2)}, u32[]{:S(2)}) collective-permute-start(bf16[128,256]{0,1:T(8,128)(2,1)S(1)} %get-tuple-element.32), channel_id=1, source_target_pairs={{4,0},{8,4},{12,8},{16,12},{20,16},{24,20},{28,24},{5,1},{9,5},{13... | collective-permute-start | bytes 196616 | tf_op jit(solution)/shard_map/ppermute | solution.py:21
  524.0 7.3 %collective-permute-start.10 = (bf16[128,256]{0,1:T(8,128)(2,1)S(1)}, bf16[128,256]{0,1:T(8,128)(2,1)S(1)}, u32[]{:S(2)}, u32[]{:S(2)}) collective-permute-start(bf16[128,256]{0,1:T(8,128)(2,1)S(1)} %get-tuple-element.31), channel_id=1, source_target_pairs={{0,4},{4,8},{8,12},{12,16},{16,20},{20,24},{24,28},{1,5},{5,9},{9,... | collective-permute-start | bytes 196616 | tf_op jit(solution)/shard_map/ppermute | solution.py:18
  546.2 51.7 %copy-start.2 = (f32[2048]{0:T(1024)S(1)}, f32[2048]{0:T(1024)}, u32[]{:S(2)}) copy-start(f32[2048]{0:T(1024)} %param.17) | copy-start | bytes 24580
Sparse Core Ops, SparseCore 0:
  9.5 46.9 all-gather.4
  58.6 42.5 all-gather.6
  103.4 58.9 all-gather.8
  164.4 58.7 all-gather.10
  229.1 70.0 reduce-scatter.3
  389.4 72.3 reduce-scatter.5
  550.8 45.5 reduce-scatter.7
